TPU v7x, 32 devices: a whole 2x2x4 slice. The times are simulated.
32 devices in a mesh: sp: 8 (over z, x), tp: 4 (over y, core).
Axes of the slice: x: 2, y: 2, z: 4, core: 2. Of those that a mesh axis runs over, the one named last changes fastest.
Arguments:
- query_proj: bfloat16 [4096, 1024], P('sp', 'tp'), may hold values from -6 to 6
- projected_keys: bfloat16 [4096, 512], P('sp', 'tp'), may hold values from -6 to 6
- projected_values: bfloat16 [4096, 512], P('sp', 'tp'), may hold values from -6 to 6
- residual: bfloat16 [4096, 2048], P(('sp', 'tp')), may hold values from -6 to 6
- out_weight: bfloat16 [1024, 2048], replicated, may hold values from -0.1875 to 0.1875
- mix_gain: float32 [2048], replicated, may hold values from 0.1 to 1.9
- norm_gain: float32 [2048], replicated, may hold values from 0.1 to 1.9
- route_expert: int32 [4096, 2], P(('sp', 'tp')), may hold values from 0 to 31, all different within a row; in each aligned block of 128 rows (0 to 127, 128 to 255, ...) at most 16 rows name the same one
- route_weight: float32 [4096, 2], P(('sp', 'tp')), may hold values from 0.2 to 1
- expert_gate: bfloat16 [32, 2048, 1024], P(('sp', 'tp')), may hold values from -0.125 to 0.125
- expert_up: bfloat16 [32, 2048, 1024], P(('sp', 'tp')), may hold values from -0.125 to 0.125
- expert_down: bfloat16 [32, 1024, 2048], P(('sp', 'tp')), may hold values from -0.1875 to 0.1875
Outputs:
- output: bfloat16 [4096, 2048], P(('sp', 'tp'))
Inputs may be any that keep to these rules, and one draw needn't show every extreme that they name: `route_expert`: each row names 2 different experts. The rows of one device (aligned blocks of 128 rows) name any one expert at most 16 times, and in some blocks some expert is named exactly 16 times.
All inputs are finite; a program needn't handle non-finite values.
Results may differ from a plain program's by a relative error of at most 0.015.
Values may be sent and summed in bfloat16 or wider, within the bound.
A program may use at most 128 MiB of HBM per device.

v0:
```python
import math
import jax
import jax.numpy as jnp
from jax import lax
from jax.sharding import PartitionSpec as P

D = 2048
HEAD_SIZE = 64
GRID_W = 64
epsilon = 1e-06
base_theta = 10000.0


def unit_length_rows(values):
    values = values.astype(jnp.float32)
    return values * lax.rsqrt(jnp.mean(values * values, axis=-1, keepdims=True) + epsilon)


def rotary_embed(head_vecs, offset):
    row_count = head_vecs.shape[0]
    quarter = head_vecs.shape[-1] // 4
    places = offset + jnp.arange(row_count, dtype=jnp.int32)
    grid_row = (places // GRID_W).astype(jnp.float32)
    grid_col = (places % GRID_W).astype(jnp.float32)
    frequency = base_theta ** (-jnp.arange(quarter, dtype=jnp.float32) / quarter)
    row_angle = grid_row[:, None, None] * frequency
    col_angle = grid_col[:, None, None] * frequency
    row_cos, row_sin = (jnp.cos(row_angle), jnp.sin(row_angle))
    col_cos, col_sin = (jnp.cos(col_angle), jnp.sin(col_angle))
    row_first = head_vecs[..., :quarter]
    row_second = head_vecs[..., quarter : 2 * quarter]
    col_first = head_vecs[..., 2 * quarter : 3 * quarter]
    col_second = head_vecs[..., 3 * quarter :]
    return jnp.concatenate(
        [
            row_first * row_cos - row_second * row_sin,
            row_second * row_cos + row_first * row_sin,
            col_first * col_cos - col_second * col_sin,
            col_second * col_cos + col_first * col_sin,
        ],
        axis=-1,
    )


def local(
    query_proj,
    projected_keys,
    projected_values,
    residual,
    out_weight,
    mix_gain,
    norm_gain,
    route_expert,
    route_weight,
    expert_gate,
    expert_up,
    expert_down,
):
    tok_count = query_proj.shape[0]
    q_heads = query_proj.shape[1] // HEAD_SIZE
    kv_heads = projected_keys.shape[1] // HEAD_SIZE
    query_group = q_heads // kv_heads
    offset = lax.axis_index("sp") * tok_count
    query_prepared = rotary_embed(
        unit_length_rows(query_proj.reshape(tok_count, q_heads, HEAD_SIZE)), offset
    ).astype(jnp.bfloat16)
    query_prepared = query_prepared.reshape(tok_count, kv_heads, query_group, HEAD_SIZE)
    key_prepared = rotary_embed(
        unit_length_rows(projected_keys.reshape(tok_count, kv_heads, HEAD_SIZE)), offset
    ).astype(jnp.bfloat16)
    v_ready = projected_values.reshape(tok_count, kv_heads, HEAD_SIZE)
    scale = HEAD_SIZE ** (-0.5)
    sums_start = jnp.zeros((tok_count, kv_heads, query_group, HEAD_SIZE), jnp.float32)
    totals_start = jnp.zeros((tok_count, kv_heads, query_group), jnp.float32)
    keys_all = lax.all_gather(key_prepared, "sp", axis=0, tiled=True)
    vals_all = lax.all_gather(v_ready, "sp", axis=0, tiled=True)
    key_count = keys_all.shape[0]
    model_width = math.gcd(key_count, 1024)
    key_blocks = keys_all.reshape(key_count // model_width, model_width, kv_heads, HEAD_SIZE)
    val_blocks = vals_all.reshape(key_count // model_width, model_width, kv_heads, HEAD_SIZE)

    def one_block(inner, pair):
        sums, totals = inner
        scores = (
            jnp.einsum(
                "thgd,nhd->thgn", query_prepared, pair[0], preferred_element_type=jnp.float32
            )
            * scale
        )
        weights = jnp.exp(scores)
        totals = totals + jnp.sum(weights, axis=-1)
        sums = sums + jnp.einsum(
            "thgn,nhd->thgd",
            weights.astype(jnp.bfloat16),
            pair[1],
            preferred_element_type=jnp.float32,
        )
        return ((sums, totals), None)

    result, unused = lax.scan(one_block, (sums_start, totals_start), (key_blocks, val_blocks))
    sums, totals = result
    attended = (
        (sums / totals[..., None]).astype(jnp.bfloat16).reshape(tok_count, q_heads * HEAD_SIZE)
    )
    by_token = lax.all_to_all(attended, "tp", split_axis=0, concat_axis=1, tiled=True)
    mixed = jnp.dot(by_token, out_weight, preferred_element_type=jnp.float32)
    stream = (residual.astype(jnp.float32) + unit_length_rows(mixed) * mix_gain).astype(
        jnp.bfloat16
    )
    normed = (unit_length_rows(stream) * norm_gain).astype(jnp.bfloat16)
    row_count = normed.shape[0]
    top_count = route_expert.shape[1]
    experts = lax.axis_size("sp") * lax.axis_size("tp")
    capacity = max(2, 2 * top_count * row_count // experts)
    flat_expert = route_expert.reshape(-1)
    onehot = (flat_expert[:, None] == jnp.arange(experts, dtype=jnp.int32)[None, :]).astype(
        jnp.int32
    )
    earlier = jnp.cumsum(onehot, axis=0) - onehot
    slot_rank = jnp.sum(earlier * onehot, axis=1)
    target = flat_expert * capacity + slot_rank
    placing = jnp.arange(experts * capacity, dtype=jnp.int32)[:, None] == target[None, :]
    placing = jnp.any(placing.reshape(experts * capacity, row_count, top_count), axis=2).astype(
        jnp.bfloat16
    )
    outgoing = jnp.dot(placing, normed, preferred_element_type=jnp.float32).astype(jnp.bfloat16)
    outgoing = outgoing.reshape(experts, capacity, D)
    gate_mat = expert_gate[0]
    up_mat = expert_up[0]
    down_mat = expert_down[0]
    slots = lax.all_to_all(outgoing, ("sp", "tp"), split_axis=0, concat_axis=0, tiled=True)
    flat_rows = slots.reshape(-1, slots.shape[-1])
    gate_pre = jnp.dot(flat_rows, gate_mat, preferred_element_type=jnp.float32)
    up_pre = jnp.dot(flat_rows, up_mat, preferred_element_type=jnp.float32)
    expert_act = (jax.nn.silu(gate_pre) * up_pre).astype(jnp.bfloat16)
    done = jnp.dot(expert_act, down_mat, preferred_element_type=jnp.float32).astype(jnp.bfloat16)
    answered = done.reshape(slots.shape)
    returned = lax.all_to_all(answered, ("sp", "tp"), split_axis=0, concat_axis=0, tiled=True)
    picked = jnp.take(returned.reshape(experts * capacity, D), target, axis=0).reshape(
        row_count, top_count, D
    )
    combined = jnp.sum(picked.astype(jnp.float32) * route_weight[:, :, None], axis=1)
    return (stream.astype(jnp.float32) + combined).astype(jnp.bfloat16)


def solution(mesh):
    return jax.shard_map(
        local,
        mesh=mesh,
        in_specs=(
            P("sp", "tp"),
            P("sp", "tp"),
            P("sp", "tp"),
            P(("sp", "tp"), None),
            P(),
            P(),
            P(),
            P(("sp", "tp"), None),
            P(("sp", "tp"), None),
            P(("sp", "tp"), None, None),
            P(("sp", "tp"), None, None),
            P(("sp", "tp"), None, None),
        ),
        out_specs=P(("sp", "tp"), None),
        check_vma=False,
    )
```

profile of v0, /device:TPU:0, one launch (start us, length us, event | category | flops | bytes accessed | tf_op | source)
XLA Modules:
  0.0 279.2 jit_solution(4073406177149737743)
XLA Ops:
  6.6 1.0 copy.72
  7.7 0.3 multiply_cosine_fusion.1
  8.0 0.7 pad_maximum_fusion.1
  8.8 1.7 copy.71
  10.5 0.8 copy.77
  11.3 0.1 eq.43
  11.4 0.1 reshape.313
  11.6 1.1 copy.73
  12.7 0.6 reduce-window.6
  13.3 0.2 slice_reduce_fusion
  13.5 0.1 fusion.37
  13.6 0.1 reduce_sum.71
  13.8 0.1 fusion.29
  13.9 0.1 convert_multiply_fusion.2
  14.0 0.1 subtract_convert_fusion.1
  14.1 37.4 %all-gather.5.cloned.1.call-done = bf16[4096,2,64]{0,2,1:T(8,128)(2,1)} async-done(((bf16[512,2,64]{0,2,1:T(8,128)(2,1)}), bf16[4096,2,64]{0,2,1:T(8,128)(2,1)}) %all-gather.5.cloned.1.call-update) | async-done | bytes 1048592 | tf_op jit(solution)/shard_map/all_gather | solution.py:75
  51.5 1.3 copy.93
  52.8 39.2 %all-gather.3.cloned.1.call-done = bf16[4096,2,64]{0,2,1:T(8,128)(2,1)} async-done(((bf16[512,2,64]{0,2,1:T(8,128)(2,1)}), bf16[4096,2,64]{0,2,1:T(8,128)(2,1)}) %all-gather.3.cloned.1.call-update) | async-done | bytes 1048592 | tf_op jit(solution)/shard_map/all_gather | solution.py:76
  92.0 1.3 copy.94
  93.3 38.0 %while.13 = (s32[]{:T(128)}, f32[512,2,2,64]{0,3,2,1:T(8,128)S(1)}, f32[512,2,2]{0,2,1:T(2,128)S(1)}, bf16[4,1024,2,64]{1,3,2,0:T(8,128)(2,1)S(1)}, bf16[4,1024,...) while((s32[]{:T(128)}, f32[512,2,2,64]{0,3,2,1:T(8,128)S(1)}, ...), condition=%wide.region_4.5_spmd.clone, body=%wide.region_2.4_spmd.clone.sunk | while | flops 545523712 | bytes 18645096 | solution.py:100
  93.4 4.6 %bitcast_reduce_fusion.2 = (f32[512,2,2]{0,2,1:T(2,128)S(1)}, f32[2,1024,512,2]{2,1,3,0:T(8,128)}) fusion(bf16[512,2,2,64]{0,3,2,1:T(8,128)(2,1)S(1)} %get-tuple-element.193, bf16[4,1024,2,64]{1,3,2,0:T(8,128)(2,1)S(1)} %get-tuple-element.192, s32[]{:T(128)} %get-tuple-element.180), kind=kOutput, calls=%fused_computation.1.clone.1 | convolution fusion | flops 272627712 | bytes 8921092 | tf_op jit(solution)/shard_map/while/body/eval_jaxpr/thgd,nhd->thgn/dot_general | solution.py:85
  98.0 4.9 %fusion.58 = f32[512,2,2,64]{0,3,2,1:T(8,128)S(1)} fusion(f32[2,1024,512,2]{2,1,3,0:T(8,128)} %get-tuple-element.170, f32[512,2,2,64]{0,3,2,1:T(8,128)S(1)} %get-tuple-element.181, bf16[4,1024,2,64]{1,3,2,0:T(8,128)(2,1)S(1)} %get-tuple-element.191, s32[]{:T(128)} %get-tuple-element.180, pred[]{:T(512)S(6)} %compare.14), kind=kOutput, calls=%fused_computation.7.clone.1 | convolution fusion | flops 272891904 | bytes 9699333 | tf_op jit(solution)/shard_map/while/body/eval_jaxpr/thgn,nhd->thgd/dot_general | solution.py:92
  102.9 4.6 %bitcast_reduce_fusion.2 = (f32[512,2,2]{0,2,1:T(2,128)S(1)}, f32[2,1024,512,2]{2,1,3,0:T(8,128)}) fusion(bf16[512,2,2,64]{0,3,2,1:T(8,128)(2,1)S(1)} %get-tuple-element.193, bf16[4,1024,2,64]{1,3,2,0:T(8,128)(2,1)S(1)} %get-tuple-element.192, s32[]{:T(128)} %get-tuple-element.180), kind=kOutput, calls=%fused_computation.1.clone.1 | convolution fusion | flops 272627712 | bytes 8921092 | tf_op jit(solution)/shard_map/while/body/eval_jaxpr/thgd,nhd->thgn/dot_general | solution.py:85
  107.5 4.9 %fusion.58 = f32[512,2,2,64]{0,3,2,1:T(8,128)S(1)} fusion(f32[2,1024,512,2]{2,1,3,0:T(8,128)} %get-tuple-element.170, f32[512,2,2,64]{0,3,2,1:T(8,128)S(1)} %get-tuple-element.181, bf16[4,1024,2,64]{1,3,2,0:T(8,128)(2,1)S(1)} %get-tuple-element.191, s32[]{:T(128)} %get-tuple-element.180, pred[]{:T(512)S(6)} %compare.14), kind=kOutput, calls=%fused_computation.7.clone.1 | convolution fusion | flops 272891904 | bytes 9699333 | tf_op jit(solution)/shard_map/while/body/eval_jaxpr/thgn,nhd->thgd/dot_general | solution.py:92
  112.4 4.6 %bitcast_reduce_fusion.2 = (f32[512,2,2]{0,2,1:T(2,128)S(1)}, f32[2,1024,512,2]{2,1,3,0:T(8,128)}) fusion(bf16[512,2,2,64]{0,3,2,1:T(8,128)(2,1)S(1)} %get-tuple-element.193, bf16[4,1024,2,64]{1,3,2,0:T(8,128)(2,1)S(1)} %get-tuple-element.192, s32[]{:T(128)} %get-tuple-element.180), kind=kOutput, calls=%fused_computation.1.clone.1 | convolution fusion | flops 272627712 | bytes 8921092 | tf_op jit(solution)/shard_map/while/body/eval_jaxpr/thgd,nhd->thgn/dot_general | solution.py:85
  117.0 4.9 %fusion.58 = f32[512,2,2,64]{0,3,2,1:T(8,128)S(1)} fusion(f32[2,1024,512,2]{2,1,3,0:T(8,128)} %get-tuple-element.170, f32[512,2,2,64]{0,3,2,1:T(8,128)S(1)} %get-tuple-element.181, bf16[4,1024,2,64]{1,3,2,0:T(8,128)(2,1)S(1)} %get-tuple-element.191, s32[]{:T(128)} %get-tuple-element.180, pred[]{:T(512)S(6)} %compare.14), kind=kOutput, calls=%fused_computation.7.clone.1 | convolution fusion | flops 272891904 | bytes 9699333 | tf_op jit(solution)/shard_map/while/body/eval_jaxpr/thgn,nhd->thgd/dot_general | solution.py:92
  121.9 4.6 %bitcast_reduce_fusion.2 = (f32[512,2,2]{0,2,1:T(2,128)S(1)}, f32[2,1024,512,2]{2,1,3,0:T(8,128)}) fusion(bf16[512,2,2,64]{0,3,2,1:T(8,128)(2,1)S(1)} %get-tuple-element.193, bf16[4,1024,2,64]{1,3,2,0:T(8,128)(2,1)S(1)} %get-tuple-element.192, s32[]{:T(128)} %get-tuple-element.180), kind=kOutput, calls=%fused_computation.1.clone.1 | convolution fusion | flops 272627712 | bytes 8921092 | tf_op jit(solution)/shard_map/while/body/eval_jaxpr/thgd,nhd->thgn/dot_general | solution.py:85
  126.5 4.9 %fusion.58 = f32[512,2,2,64]{0,3,2,1:T(8,128)S(1)} fusion(f32[2,1024,512,2]{2,1,3,0:T(8,128)} %get-tuple-element.170, f32[512,2,2,64]{0,3,2,1:T(8,128)S(1)} %get-tuple-element.181, bf16[4,1024,2,64]{1,3,2,0:T(8,128)(2,1)S(1)} %get-tuple-element.191, s32[]{:T(128)} %get-tuple-element.180, pred[]{:T(512)S(6)} %compare.14), kind=kOutput, calls=%fused_computation.7.clone.1 | convolution fusion | flops 272891904 | bytes 9699333 | tf_op jit(solution)/shard_map/while/body/eval_jaxpr/thgn,nhd->thgd/dot_general | solution.py:92
  131.5 0.1 all_to_all.20
  131.5 0.7 copy.76
  132.3 3.5 %all-to-all-start = ((bf16[4,128,256]{1,2,0:T(8,128)(2,1)}), bf16[4,128,256]{1,2,0:T(8,128)(2,1)S(1)}, u32[]{:S(2)}, u32[]{:S(2)}) async-start(bf16[4,128,256]{1,2,0:T(8,128)(2,1)} %copy.76), calls=%async_computation | async-start | bytes 524288 | tf_op jit(solution)/shard_map/all_to_all | solution.py:105
  135.9 5.9 %all-to-all-done = bf16[4,128,256]{1,2,0:T(8,128)(2,1)S(1)} async-done(((bf16[4,128,256]{1,2,0:T(8,128)(2,1)}), bf16[4,128,256]{1,2,0:T(8,128)(2,1)S(1)}, u32[]{:S(2)}, u32[]{:S(2)}) %all-to-all-start) | async-done | bytes 262176 | tf_op jit(solution)/shard_map/all_to_all | solution.py:105
  141.8 3.0 %multiply_reduce_fusion.1 = (f32[128]{0:T(128)S(1)}, f32[128,2048]{1,0:T(8,128)S(1)}) fusion(bf16[128,1024]{0,1:T(8,128)(2,1)S(1)} %bitcast.119, bf16[1024,2048]{1,0:T(8,128)(2,1)} %param.18), kind=kOutput, calls=%fused_computation.38 | convolution fusion | flops 537395072 | bytes 5505536 | tf_op jit(solution)/shard_map/dot_general | solution.py:106
  144.8 0.4 fusion.23
  145.2 0.8 convolution_convert_fusion
  146.0 51.2 %all_to_all.29 = bf16[32,16,2048]{2,1,0:T(8,128)(2,1)S(1)} all-to-all(bf16[32,16,2048]{2,1,0:T(8,128)(2,1)S(1)} %bitcast.113), channel_id=1, replica_groups=mesh['sp'=8,'tp'=4] {'sp','tp'}, dimensions={0} | all-to-all | bytes 4194304 | tf_op jit(solution)/shard_map/all_to_all | solution.py:131
  197.2 3.7 %fusion.16 = f32[512,1024]{1,0:T(8,128)} fusion(bf16[512,2048]{1,0:T(8,128)(2,1)S(1)} %bitcast.117, bf16[1,2048,1024]{2,1,0:T(8,128)(2,1)S(1)} %copy-done.5), kind=kOutput, calls=%fused_computation.21 | convolution fusion | flops 2147483648 | bytes 8388608 | tf_op jit(solution)/shard_map/dot_general | solution.py:133
  200.9 9.9 %fusion.18 = bf16[512,2048]{1,0:T(8,128)(2,1)} fusion(bf16[1,1024,2048]{2,1,0:T(8,128)(2,1)} %param.25, f32[512,1024]{1,0:T(8,128)} %fusion.16, bf16[512,2048]{1,0:T(8,128)(2,1)S(1)} %bitcast.118, bf16[1,2048,1024]{2,1,0:T(8,128)(2,1)} %param.24), kind=kOutput, calls=%fused_computation.23 | convolution fusion | flops 4299161600 | bytes 14680064 | tf_op jit(solution)/shard_map/dot_general | solution.py:136
  210.8 3.7 %all-to-all-start.2 = ((bf16[32,16,2048]{2,1,0:T(8,128)(2,1)}), bf16[32,16,2048]{2,1,0:T(8,128)(2,1)S(1)}, u32[]{:S(2)}, u32[]{:S(2)}) async-start(bf16[32,16,2048]{2,1,0:T(8,128)(2,1)} %bitcast.116), calls=%async_computation.2 | async-start | bytes 4194304 | tf_op jit(solution)/shard_map/all_to_all | solution.py:138
  214.5 0.1 copy.82
  214.7 0.1 mul.327
  214.8 0.1 copy.81
  214.9 0.1 copy.83
  215.1 48.2 %all-to-all-done.2 = bf16[32,16,2048]{2,1,0:T(8,128)(2,1)S(1)} async-done(((bf16[32,16,2048]{2,1,0:T(8,128)(2,1)}), bf16[32,16,2048]{2,1,0:T(8,128)(2,1)S(1)}, u32[]{:S(2)}, u32[]{:S(2)}) %all-to-all-start.2) | async-done | bytes 2097184 | tf_op jit(solution)/shard_map/all_to_all | solution.py:138
  263.2 2.3 gather_fusion
  265.6 1.7 gather.7
  267.3 4.1 %multiply_reduce_fusion = f32[128,2048]{1,0:T(8,128)S(1)} fusion(bf16[128,2,2048]{2,1,0:T(2,128)(2,1)S(1)} %gather.7, pred[128,2]{1,0:T(8,128)(4,1)S(1)} %copy.81, f32[128,2]{1,0:T(8,128)S(1)} %copy.83), kind=kLoop, calls=%fused_computation.25 | loop fusion | flops 1835008 | bytes 2098432 | tf_op jit(solution)/shard_map/reduce_sum | solution.py:142
  271.4 0.9 fusion.26
  (42 shorter events, 0.6 us)
Async XLA Ops:
  6.5 45.0 %all-gather.5.cloned.1.call-start = ((), (), s32[]{:S(2)}) async-start(), calls=%async_computation.4 | async-start | bytes 1179648 | tf_op jit(solution)/shard_map/all_gather | solution.py:75
  8.7 83.3 %all-gather.3.cloned.1.call-start = ((), (), s32[]{:S(2)}) async-start(), calls=%async_computation.3 | async-start | bytes 1179648 | tf_op jit(solution)/shard_map/all_gather | solution.py:76
  93.3 42.5 %copy-start.1 = (s32[128,2]{0,1:T(2,128)S(1)}, s32[128,2]{0,1:T(2,128)}, u32[]{:S(2)}) copy-start(s32[128,2]{0,1:T(2,128)} %param.21) | copy-start | bytes 3076
  131.4 13.4 %copy-start = (bf16[128,2048]{1,0:T(8,128)(2,1)S(1)}, bf16[128,2048]{1,0:T(8,128)(2,1)}, u32[]{:S(2)}) copy-start(bf16[128,2048]{1,0:T(8,128)(2,1)} %param.17) | copy-start | bytes 1572868
  131.4 13.4 %copy-start.2 = (f32[2048]{0:T(1024)S(1)}, f32[2048]{0:T(1024)}, u32[]{:S(2)}) copy-start(f32[2048]{0:T(1024)} %param.19) | copy-start | bytes 24580
  132.3 13.0 %copy-start.3 = (f32[2048]{0:T(1024)S(1)}, f32[2048]{0:T(1024)}, u32[]{:S(2)}) copy-start(f32[2048]{0:T(1024)} %param.20) | copy-start | bytes 24580
  132.3 9.5 %all-to-all-start = ((bf16[4,128,256]{1,2,0:T(8,128)(2,1)}), bf16[4,128,256]{1,2,0:T(8,128)(2,1)S(1)}, u32[]{:S(2)}, u32[]{:S(2)}) async-start(bf16[4,128,256]{1,2,0:T(8,128)(2,1)} %copy.76), calls=%async_computation | async-start | bytes 524288 | tf_op jit(solution)/shard_map/all_to_all | solution.py:105
  144.8 52.4 %copy-start.5 = (bf16[1,2048,1024]{2,1,0:T(8,128)(2,1)S(1)}, bf16[1,2048,1024]{2,1,0:T(8,128)(2,1)}, u32[]{:S(2)}) copy-start(bf16[1,2048,1024]{2,1,0:T(8,128)(2,1)} %param.23) | copy-start | bytes 12582916
  210.8 4.1 %copy-start.4 = (f32[128,2]{0,1:T(2,128)S(1)}, f32[128,2]{0,1:T(2,128)}, u32[]{:S(2)}) copy-start(f32[128,2]{0,1:T(2,128)} %param.22) | copy-start | bytes 3076
  210.8 52.4 %all-to-all-start.2 = ((bf16[32,16,2048]{2,1,0:T(8,128)(2,1)}), bf16[32,16,2048]{2,1,0:T(8,128)(2,1)S(1)}, u32[]{:S(2)}, u32[]{:S(2)}) async-start(bf16[32,16,2048]{2,1,0:T(8,128)(2,1)} %bitcast.116), calls=%async_computation.2 | async-start | bytes 4194304 | tf_op jit(solution)/shard_map/all_to_all | solution.py:138
Sparse Core Ops, SparseCore 0:
  9.4 42.1 all-gather.4
  53.6 38.3 all-gather.2
where the time goes:
time: 280 us; the launch traced here: 279 us
  waiting for transfers between devices  131 us (47%)
  matrix products  55.3 us (20%)
  blocking collectives  51.2 us (18%)
  between operations  13.7 us (5%)
  local copies, waits for them, and re-layouts  13.3 us (5%)
  other arithmetic  7.73 us (3%)
  starting transfers between devices  7.26 us (3%)
    all_to_all x1, blocking collectives, local(): lax.all_to_all(outgoing, ('sp', 'tp'), split_axis=0, concat_axis=0, tiled...  51.2 us
    all_to_all x1, waiting for transfers between devices, local(): lax.all_to_all(answered, ('sp', 'tp'), split_axis=0, concat_axis=0, tiled...  48.2 us
    all_gather x1, waiting for transfers between devices, local(): vals_all = lax.all_gather(v_ready, 'sp', axis=0, tiled=True)  39.2 us
    all_gather x1, waiting for transfers between devices, local(): keys_all = lax.all_gather(key_prepared, 'sp', axis=0, tiled=True)  37.4 us
    dot_general x4, matrix products, one_block(): jnp.einsum('thgn,nhd->thgd', weights.astype(jnp.bfloat16), pair[1], prefe...  19.4 us
    dot_general x4, matrix products, one_block(): jnp.einsum('thgd,nhd->thgn', query_prepared, pair[0], preferred_element_t...  18.4 us
    dot_general x1, matrix products, local(): jnp.dot(expert_act, down_mat, preferred_element_type=jnp.float32)  9.89 us
    all_to_all x1, waiting for transfers between devices, local(): lax.all_to_all(attended, 'tp', split_axis=0, concat_axis=1, tiled=True)  5.88 us
  transfers between devices with their start and end apart: 4, of which 4 were waited for; matrix products, arithmetic and copies ran while one was open for 3% of the time, Pallas kernels for 0%

commit v1 on v0

--- a/solution.py
+++ b/solution.py
@@ -72,7 +72,12 @@
     scale = HEAD_SIZE ** (-0.5)
     sums_start = jnp.zeros((tok_count, kv_heads, query_group, HEAD_SIZE), jnp.float32)
     totals_start = jnp.zeros((tok_count, kv_heads, query_group), jnp.float32)
-    keys_all = lax.all_gather(key_prepared, "sp", axis=0, tiled=True)
+    ring = [key_prepared]
+    for hop in range(7):
+        ring.append(lax.ppermute(ring[-1], "sp", [(dev, (dev + 1) % 8) for dev in range(8)]))
+    keys_all = jnp.roll(
+        jnp.concatenate(ring[::-1], axis=0), (lax.axis_index("sp") + 1) * ring[0].shape[0], axis=0
+    )
     vals_all = lax.all_gather(v_ready, "sp", axis=0, tiled=True)
     key_count = keys_all.shape[0]
     model_width = math.gcd(key_count, 1024)

time: 280 us -> 255 us (0.911)
  waiting for transfers between devices: 131 us -> 106 us
  starting transfers between devices: 7.26 us -> 10.5 us
    ppermute x0 -> x7, waiting for transfers between devices: none -> 51.7 us  [local(): lax.ppermute(ring[-1], 'sp', [(dev, (dev + 1) % 8) for dev in range(8)])]
    all_gather x1, waiting for transfers between devices: 39.2 us -> 0.02 us  [local(): vals_all = lax.all_gather(v_ready, 'sp', axis=0, tiled=True)]
    all_gather x1 -> x0, waiting for transfers between devices: 37.4 us -> none  [local(): keys_all = lax.all_gather(key_prepared, 'sp', axis=0, tiled=True)]
    ppermute x0 -> x7, starting transfers between devices: none -> 3.49 us  [local(): lax.ppermute(ring[-1], 'sp', [(dev, (dev + 1) % 8) for dev in range(8)])]
  transfers between devices with their start and end apart: 4 -> 10, of which waited for: 4 -> 9; matrix products, arithmetic and copies ran while one was open for 3% -> 2% of each run, Pallas kernels for 0% -> 0%
where the time goes in v1:
time: 255 us; the launch traced here: 254 us
  waiting for transfers between devices  106 us (42%)
  matrix products  55.3 us (22%)
  blocking collectives  50.7 us (20%)
  between operations  13.9 us (5%)
  local copies, waits for them, and re-layouts  10.9 us (4%)
  starting transfers between devices  10.5 us (4%)
  other arithmetic  7.08 us (3%)
    ppermute x7, waiting for transfers between devices, local(): lax.ppermute(ring[-1], 'sp', [(dev, (dev + 1) % 8) for dev in range(8)])  51.7 us
    all_to_all x1, blocking collectives, local(): lax.all_to_all(outgoing, ('sp', 'tp'), split_axis=0, concat_axis=0, tiled...  50.7 us
    all_to_all x1, waiting for transfers between devices, local(): lax.all_to_all(answered, ('sp', 'tp'), split_axis=0, concat_axis=0, tiled...  48.2 us
    dot_general x4, matrix products, one_block(): jnp.einsum('thgn,nhd->thgd', weights.astype(jnp.bfloat16), pair[1], prefe...  19.4 us
    dot_general x4, matrix products, one_block(): jnp.einsum('thgd,nhd->thgn', query_prepared, pair[0], preferred_element_t...  18.4 us
    dot_general x1, matrix products, local(): jnp.dot(expert_act, down_mat, preferred_element_type=jnp.float32)  9.89 us
    all_to_all x1, waiting for transfers between devices, local(): lax.all_to_all(attended, 'tp', split_axis=0, concat_axis=1, tiled=True)  5.89 us
  transfers between devices with their start and end apart: 10, of which 9 were waited for; matrix products, arithmetic and copies ran while one was open for 2% of the time, Pallas kernels for 0%

profile of v1, /device:TPU:0, one launch (start us, length us, event | category | flops | bytes accessed | tf_op | source)
XLA Modules:
  0.0 254.3 jit_solution(6639145262729813667)
XLA Ops:
  6.6 1.0 copy.72
  7.7 0.3 multiply_cosine_fusion.1
  8.1 3.0 %collective-permute-start = (bf16[512,2,64]{0,2,1:T(8,128)(2,1)S(1)}, bf16[512,2,64]{0,2,1:T(8,128)(2,1)S(1)}, u32[]{:S(2)}, u32[]{:S(2)}) collective-permute-start(bf16[512,2,64]{0,2,1:T(8,128)(2,1)S(1)} %pad_maximum_fusion.1), channel_id=1, source_target_pairs={{0,4},{4,8},{8,12},{12,16},{16,20},{20,24},{24,28},{28,0},{1,5},{5... | collective-permute-start | bytes 393224 | tf_op jit(solution)/shard_map/ppermute | solution.py:77
  11.1 1.7 copy.71
  12.8 0.1 copy.77
  12.9 0.1 eq.46
  13.1 4.6 %collective-permute-done = bf16[512,2,64]{0,2,1:T(8,128)(2,1)S(1)} collective-permute-done((bf16[512,2,64]{0,2,1:T(8,128)(2,1)S(1)}, bf16[512,2,64]{0,2,1:T(8,128)(2,1)S(1)}, u32[]{:S(2)}, u32[]{:S(2)}) %collective-permute-start) | collective-permute-done | bytes 131104 | tf_op jit(solution)/shard_map/ppermute | solution.py:77
  17.7 0.6 reduce-window.6
  18.3 7.2 %collective-permute-done.1 = bf16[512,2,64]{0,2,1:T(8,128)(2,1)S(1)} collective-permute-done((bf16[512,2,64]{0,2,1:T(8,128)(2,1)S(1)}, bf16[512,2,64]{0,2,1:T(8,128)(2,1)S(1)}, u32[]{:S(2)}, u32[]{:S(2)}) %collective-permute-start.1) | collective-permute-done | bytes 131104 | tf_op jit(solution)/shard_map/ppermute | solution.py:77
  25.4 0.2 slice_reduce_fusion
  25.6 0.1 reshape.313
  25.8 0.1 copy.73
  26.0 7.8 %collective-permute-done.2 = bf16[512,2,64]{0,2,1:T(8,128)(2,1)S(1)} collective-permute-done((bf16[512,2,64]{0,2,1:T(8,128)(2,1)S(1)}, bf16[512,2,64]{0,2,1:T(8,128)(2,1)S(1)}, u32[]{:S(2)}, u32[]{:S(2)}) %collective-permute-start.2) | collective-permute-done | bytes 131104 | tf_op jit(solution)/shard_map/ppermute | solution.py:77
  33.8 7.6 %collective-permute-done.3 = bf16[512,2,64]{0,2,1:T(8,128)(2,1)S(1)} collective-permute-done((bf16[512,2,64]{0,2,1:T(8,128)(2,1)S(1)}, bf16[512,2,64]{0,2,1:T(8,128)(2,1)S(1)}, u32[]{:S(2)}, u32[]{:S(2)}) %collective-permute-start.3) | collective-permute-done | bytes 131104 | tf_op jit(solution)/shard_map/ppermute | solution.py:77
  41.5 8.1 %collective-permute-done.4 = bf16[512,2,64]{0,2,1:T(8,128)(2,1)S(1)} collective-permute-done((bf16[512,2,64]{0,2,1:T(8,128)(2,1)S(1)}, bf16[512,2,64]{0,2,1:T(8,128)(2,1)S(1)}, u32[]{:S(2)}, u32[]{:S(2)}) %collective-permute-start.4) | collective-permute-done | bytes 131104 | tf_op jit(solution)/shard_map/ppermute | solution.py:77
  49.6 0.5 collective-permute-start.5
  50.2 9.2 %collective-permute-done.5 = bf16[512,2,64]{0,2,1:T(8,128)(2,1)S(1)} collective-permute-done((bf16[512,2,64]{0,2,1:T(8,128)(2,1)S(1)}, bf16[512,2,64]{0,2,1:T(8,128)(2,1)S(1)}, u32[]{:S(2)}, u32[]{:S(2)}) %collective-permute-start.5) | collective-permute-done | bytes 131104 | tf_op jit(solution)/shard_map/ppermute | solution.py:77
  59.5 0.1 reduce_sum.71
  59.7 7.3 %collective-permute-done.6 = bf16[512,2,64]{0,2,1:T(8,128)(2,1)S(1)} collective-permute-done((bf16[512,2,64]{0,2,1:T(8,128)(2,1)S(1)}, bf16[512,2,64]{0,2,1:T(8,128)(2,1)S(1)}, u32[]{:S(2)}, u32[]{:S(2)}) %collective-permute-start.6) | collective-permute-done | bytes 131104 | tf_op jit(solution)/shard_map/ppermute | solution.py:77
  67.5 1.3 copy.94
  68.8 38.0 %while.13 = (s32[]{:T(128)}, f32[512,2,2,64]{0,3,2,1:T(8,128)S(1)}, f32[512,2,2]{0,2,1:T(2,128)S(1)}, bf16[4,1024,2,64]{1,3,2,0:T(8,128)(2,1)S(1)}, bf16[4,1024,...) while((s32[]{:T(128)}, f32[512,2,2,64]{0,3,2,1:T(8,128)S(1)}, ...), condition=%wide.region_4.5_spmd.clone, body=%wide.region_2.4_spmd.clone.sunk | while | flops 545523712 | bytes 18645096 | solution.py:105
  68.9 4.6 %bitcast_reduce_fusion.2 = (f32[512,2,2]{0,2,1:T(2,128)S(1)}, f32[2,1024,512,2]{2,1,3,0:T(8,128)}) fusion(bf16[512,2,2,64]{0,3,2,1:T(8,128)(2,1)S(1)} %get-tuple-element.193, bf16[4,1024,2,64]{1,3,2,0:T(8,128)(2,1)S(1)} %get-tuple-element.192, s32[]{:T(128)} %get-tuple-element.180), kind=kOutput, calls=%fused_computation.1.clone.1 | convolution fusion | flops 272627712 | bytes 8921092 | tf_op jit(solution)/shard_map/while/body/eval_jaxpr/thgd,nhd->thgn/dot_general | solution.py:90
  73.5 4.9 %fusion.58 = f32[512,2,2,64]{0,3,2,1:T(8,128)S(1)} fusion(f32[2,1024,512,2]{2,1,3,0:T(8,128)} %get-tuple-element.170, f32[512,2,2,64]{0,3,2,1:T(8,128)S(1)} %get-tuple-element.181, bf16[4,1024,2,64]{1,3,2,0:T(8,128)(2,1)S(1)} %get-tuple-element.191, s32[]{:T(128)} %get-tuple-element.180, pred[]{:T(512)S(6)} %compare.15), kind=kOutput, calls=%fused_computation.7.clone.1 | convolution fusion | flops 272891904 | bytes 9699333 | tf_op jit(solution)/shard_map/while/body/eval_jaxpr/thgn,nhd->thgd/dot_general | solution.py:97
  78.4 4.6 %bitcast_reduce_fusion.2 = (f32[512,2,2]{0,2,1:T(2,128)S(1)}, f32[2,1024,512,2]{2,1,3,0:T(8,128)}) fusion(bf16[512,2,2,64]{0,3,2,1:T(8,128)(2,1)S(1)} %get-tuple-element.193, bf16[4,1024,2,64]{1,3,2,0:T(8,128)(2,1)S(1)} %get-tuple-element.192, s32[]{:T(128)} %get-tuple-element.180), kind=kOutput, calls=%fused_computation.1.clone.1 | convolution fusion | flops 272627712 | bytes 8921092 | tf_op jit(solution)/shard_map/while/body/eval_jaxpr/thgd,nhd->thgn/dot_general | solution.py:90
  83.0 4.9 %fusion.58 = f32[512,2,2,64]{0,3,2,1:T(8,128)S(1)} fusion(f32[2,1024,512,2]{2,1,3,0:T(8,128)} %get-tuple-element.170, f32[512,2,2,64]{0,3,2,1:T(8,128)S(1)} %get-tuple-element.181, bf16[4,1024,2,64]{1,3,2,0:T(8,128)(2,1)S(1)} %get-tuple-element.191, s32[]{:T(128)} %get-tuple-element.180, pred[]{:T(512)S(6)} %compare.15), kind=kOutput, calls=%fused_computation.7.clone.1 | convolution fusion | flops 272891904 | bytes 9699333 | tf_op jit(solution)/shard_map/while/body/eval_jaxpr/thgn,nhd->thgd/dot_general | solution.py:97
  87.9 4.6 %bitcast_reduce_fusion.2 = (f32[512,2,2]{0,2,1:T(2,128)S(1)}, f32[2,1024,512,2]{2,1,3,0:T(8,128)}) fusion(bf16[512,2,2,64]{0,3,2,1:T(8,128)(2,1)S(1)} %get-tuple-element.193, bf16[4,1024,2,64]{1,3,2,0:T(8,128)(2,1)S(1)} %get-tuple-element.192, s32[]{:T(128)} %get-tuple-element.180), kind=kOutput, calls=%fused_computation.1.clone.1 | convolution fusion | flops 272627712 | bytes 8921092 | tf_op jit(solution)/shard_map/while/body/eval_jaxpr/thgd,nhd->thgn/dot_general | solution.py:90
  92.5 4.9 %fusion.58 = f32[512,2,2,64]{0,3,2,1:T(8,128)S(1)} fusion(f32[2,1024,512,2]{2,1,3,0:T(8,128)} %get-tuple-element.170, f32[512,2,2,64]{0,3,2,1:T(8,128)S(1)} %get-tuple-element.181, bf16[4,1024,2,64]{1,3,2,0:T(8,128)(2,1)S(1)} %get-tuple-element.191, s32[]{:T(128)} %get-tuple-element.180, pred[]{:T(512)S(6)} %compare.15), kind=kOutput, calls=%fused_computation.7.clone.1 | convolution fusion | flops 272891904 | bytes 9699333 | tf_op jit(solution)/shard_map/while/body/eval_jaxpr/thgn,nhd->thgd/dot_general | solution.py:97
  97.4 4.6 %bitcast_reduce_fusion.2 = (f32[512,2,2]{0,2,1:T(2,128)S(1)}, f32[2,1024,512,2]{2,1,3,0:T(8,128)}) fusion(bf16[512,2,2,64]{0,3,2,1:T(8,128)(2,1)S(1)} %get-tuple-element.193, bf16[4,1024,2,64]{1,3,2,0:T(8,128)(2,1)S(1)} %get-tuple-element.192, s32[]{:T(128)} %get-tuple-element.180), kind=kOutput, calls=%fused_computation.1.clone.1 | convolution fusion | flops 272627712 | bytes 8921092 | tf_op jit(solution)/shard_map/while/body/eval_jaxpr/thgd,nhd->thgn/dot_general | solution.py:90
  102.0 4.9 %fusion.58 = f32[512,2,2,64]{0,3,2,1:T(8,128)S(1)} fusion(f32[2,1024,512,2]{2,1,3,0:T(8,128)} %get-tuple-element.170, f32[512,2,2,64]{0,3,2,1:T(8,128)S(1)} %get-tuple-element.181, bf16[4,1024,2,64]{1,3,2,0:T(8,128)(2,1)S(1)} %get-tuple-element.191, s32[]{:T(128)} %get-tuple-element.180, pred[]{:T(512)S(6)} %compare.15), kind=kOutput, calls=%fused_computation.7.clone.1 | convolution fusion | flops 272891904 | bytes 9699333 | tf_op jit(solution)/shard_map/while/body/eval_jaxpr/thgn,nhd->thgd/dot_general | solution.py:97
  107.0 0.7 copy.76
  107.8 3.4 %all-to-all-start = ((bf16[4,128,256]{1,2,0:T(8,128)(2,1)}), bf16[4,128,256]{1,2,0:T(8,128)(2,1)S(1)}, u32[]{:S(2)}, u32[]{:S(2)}) async-start(bf16[4,128,256]{1,2,0:T(8,128)(2,1)} %copy.76), calls=%async_computation | async-start | bytes 524288 | tf_op jit(solution)/shard_map/all_to_all | solution.py:110
  111.3 5.9 %all-to-all-done = bf16[4,128,256]{1,2,0:T(8,128)(2,1)S(1)} async-done(((bf16[4,128,256]{1,2,0:T(8,128)(2,1)}), bf16[4,128,256]{1,2,0:T(8,128)(2,1)S(1)}, u32[]{:S(2)}, u32[]{:S(2)}) %all-to-all-start) | async-done | bytes 262176 | tf_op jit(solution)/shard_map/all_to_all | solution.py:110
  117.2 3.1 %multiply_reduce_fusion.1 = (f32[128]{0:T(128)S(1)}, f32[128,2048]{1,0:T(8,128)S(1)}) fusion(bf16[128,1024]{0,1:T(8,128)(2,1)S(1)} %bitcast.120, bf16[1024,2048]{1,0:T(8,128)(2,1)} %param.18), kind=kOutput, calls=%fused_computation.38 | convolution fusion | flops 537395072 | bytes 5505536 | tf_op jit(solution)/shard_map/dot_general | solution.py:111
  120.3 0.4 fusion.23
  120.6 0.3 copy-done.4
  120.9 0.8 convolution_convert_fusion
  121.7 50.7 %all_to_all.29 = bf16[32,16,2048]{2,1,0:T(8,128)(2,1)S(1)} all-to-all(bf16[32,16,2048]{2,1,0:T(8,128)(2,1)S(1)} %bitcast.113), channel_id=1, replica_groups=mesh['sp'=8,'tp'=4] {'sp','tp'}, dimensions={0} | all-to-all | bytes 4194304 | tf_op jit(solution)/shard_map/all_to_all | solution.py:136
  172.4 3.7 %fusion.16 = f32[512,1024]{1,0:T(8,128)} fusion(bf16[512,2048]{1,0:T(8,128)(2,1)S(1)} %bitcast.118, bf16[1,2048,1024]{2,1,0:T(8,128)(2,1)S(1)} %copy-done.6), kind=kOutput, calls=%fused_computation.21 | convolution fusion | flops 2147483648 | bytes 8388608 | tf_op jit(solution)/shard_map/dot_general | solution.py:138
  176.1 9.9 %fusion.18 = bf16[512,2048]{1,0:T(8,128)(2,1)} fusion(bf16[1,1024,2048]{2,1,0:T(8,128)(2,1)} %param.25, f32[512,1024]{1,0:T(8,128)} %fusion.16, bf16[512,2048]{1,0:T(8,128)(2,1)S(1)} %bitcast.119, bf16[1,2048,1024]{2,1,0:T(8,128)(2,1)} %param.24), kind=kOutput, calls=%fused_computation.23 | convolution fusion | flops 4299161600 | bytes 14680064 | tf_op jit(solution)/shard_map/dot_general | solution.py:141
  186.0 3.6 %all-to-all-start.2 = ((bf16[32,16,2048]{2,1,0:T(8,128)(2,1)}), bf16[32,16,2048]{2,1,0:T(8,128)(2,1)S(1)}, u32[]{:S(2)}, u32[]{:S(2)}) async-start(bf16[32,16,2048]{2,1,0:T(8,128)(2,1)} %bitcast.117), calls=%async_computation.2 | async-start | bytes 4194304 | tf_op jit(solution)/shard_map/all_to_all | solution.py:143
  189.6 0.1 copy.82
  189.7 0.1 mul.331
  189.9 0.1 copy.81
  190.2 48.2 %all-to-all-done.2 = bf16[32,16,2048]{2,1,0:T(8,128)(2,1)S(1)} async-done(((bf16[32,16,2048]{2,1,0:T(8,128)(2,1)}), bf16[32,16,2048]{2,1,0:T(8,128)(2,1)S(1)}, u32[]{:S(2)}, u32[]{:S(2)}) %all-to-all-start.2) | async-done | bytes 2097184 | tf_op jit(solution)/shard_map/all_to_all | solution.py:143
  238.3 2.3 gather_fusion
  240.7 1.7 gather.7
  242.4 4.1 %multiply_reduce_fusion = f32[128,2048]{1,0:T(8,128)S(1)} fusion(bf16[128,2,2048]{2,1,0:T(2,128)(2,1)S(1)} %gather.7, pred[128,2]{1,0:T(8,128)(4,1)S(1)} %copy.81, f32[128,2]{1,0:T(8,128)S(1)} %copy.83), kind=kLoop, calls=%fused_computation.25 | loop fusion | flops 1835008 | bytes 2098432 | tf_op jit(solution)/shard_map/reduce_sum | solution.py:147
  246.5 0.9 fusion.26
  (72 shorter events, 1.4 us)
Async XLA Ops:
  6.5 6.3 %copy-start.2 = (s32[128,2]{0,1:T(2,128)S(1)}, s32[128,2]{0,1:T(2,128)}, u32[]{:S(2)}) copy-start(s32[128,2]{0,1:T(2,128)} %param.21) | copy-start | bytes 3076
  6.5 19.2 %copy-start.1 = (bf16[512,256]{1,0:T(8,128)(2,1)S(1)}, bf16[512,256]{1,0:T(8,128)(2,1)}, u32[]{:S(2)}) copy-start(bf16[512,256]{1,0:T(8,128)(2,1)} %param.14) | copy-start | bytes 786436
  6.5 61.0 %all-gather.2.cloned.1.call-start = ((), (), s32[]{:S(2)}) async-start(), calls=%async_computation.3 | async-start | bytes 1179648 | tf_op jit(solution)/shard_map/all_gather | solution.py:81
  8.1 9.6 %collective-permute-start = (bf16[512,2,64]{0,2,1:T(8,128)(2,1)S(1)}, bf16[512,2,64]{0,2,1:T(8,128)(2,1)S(1)}, u32[]{:S(2)}, u32[]{:S(2)}) collective-permute-start(bf16[512,2,64]{0,2,1:T(8,128)(2,1)S(1)} %pad_maximum_fusion.1), channel_id=1, source_target_pairs={{0,4},{4,8},{8,12},{12,16},{16,20},{20,24},{24,28},{28,0},{1,5},{5... | collective-permute-start | bytes 393224 | tf_op jit(solution)/shard_map/ppermute | solution.py:77
  17.7 7.8 %collective-permute-start.1 = (bf16[512,2,64]{0,2,1:T(8,128)(2,1)S(1)}, bf16[512,2,64]{0,2,1:T(8,128)(2,1)S(1)}, u32[]{:S(2)}, u32[]{:S(2)}) collective-permute-start(bf16[512,2,64]{0,2,1:T(8,128)(2,1)S(1)} %collective-permute-done), channel_id=1, source_target_pairs={{0,4},{4,8},{8,12},{12,16},{16,20},{20,24},{24,28},{28,0},{1,5},{5... | collective-permute-start | bytes 393224 | tf_op jit(solution)/shard_map/ppermute | solution.py:77
  25.4 8.4 %collective-permute-start.2 = (bf16[512,2,64]{0,2,1:T(8,128)(2,1)S(1)}, bf16[512,2,64]{0,2,1:T(8,128)(2,1)S(1)}, u32[]{:S(2)}, u32[]{:S(2)}) collective-permute-start(bf16[512,2,64]{0,2,1:T(8,128)(2,1)S(1)} %collective-permute-done.1), channel_id=1, source_target_pairs={{0,4},{4,8},{8,12},{12,16},{16,20},{20,24},{24,28},{28,0},{1,5},{5... | collective-permute-start | bytes 393224 | tf_op jit(solution)/shard_map/ppermute | solution.py:77
  33.8 7.7 %collective-permute-start.3 = (bf16[512,2,64]{0,2,1:T(8,128)(2,1)S(1)}, bf16[512,2,64]{0,2,1:T(8,128)(2,1)S(1)}, u32[]{:S(2)}, u32[]{:S(2)}) collective-permute-start(bf16[512,2,64]{0,2,1:T(8,128)(2,1)S(1)} %collective-permute-done.2), channel_id=1, source_target_pairs={{0,4},{4,8},{8,12},{12,16},{16,20},{20,24},{24,28},{28,0},{1,5},{5... | collective-permute-start | bytes 393224 | tf_op jit(solution)/shard_map/ppermute | solution.py:77
  41.5 8.2 %collective-permute-start.4 = (bf16[512,2,64]{0,2,1:T(8,128)(2,1)S(1)}, bf16[512,2,64]{0,2,1:T(8,128)(2,1)S(1)}, u32[]{:S(2)}, u32[]{:S(2)}) collective-permute-start(bf16[512,2,64]{0,2,1:T(8,128)(2,1)S(1)} %collective-permute-done.3), channel_id=1, source_target_pairs={{0,4},{4,8},{8,12},{12,16},{16,20},{20,24},{24,28},{28,0},{1,5},{5... | collective-permute-start | bytes 393224 | tf_op jit(solution)/shard_map/ppermute | solution.py:77
  49.6 9.7 %collective-permute-start.5 = (bf16[512,2,64]{0,2,1:T(8,128)(2,1)S(1)}, bf16[512,2,64]{0,2,1:T(8,128)(2,1)S(1)}, u32[]{:S(2)}, u32[]{:S(2)}) collective-permute-start(bf16[512,2,64]{0,2,1:T(8,128)(2,1)S(1)} %collective-permute-done.4), channel_id=1, source_target_pairs={{0,4},{4,8},{8,12},{12,16},{16,20},{20,24},{24,28},{28,0},{1,5},{5... | collective-permute-start | bytes 393224 | tf_op jit(solution)/shard_map/ppermute | solution.py:77
  59.4 7.7 %collective-permute-start.6 = (bf16[512,2,64]{0,2,1:T(8,128)(2,1)S(1)}, bf16[512,2,64]{0,2,1:T(8,128)(2,1)S(1)}, u32[]{:S(2)}, u32[]{:S(2)}) collective-permute-start(bf16[512,2,64]{0,2,1:T(8,128)(2,1)S(1)} %collective-permute-done.5), channel_id=1, source_target_pairs={{0,4},{4,8},{8,12},{12,16},{16,20},{20,24},{24,28},{28,0},{1,5},{5... | collective-permute-start | bytes 393224 | tf_op jit(solution)/shard_map/ppermute | solution.py:77
  107.8 9.4 %all-to-all-start = ((bf16[4,128,256]{1,2,0:T(8,128)(2,1)}), bf16[4,128,256]{1,2,0:T(8,128)(2,1)S(1)}, u32[]{:S(2)}, u32[]{:S(2)}) async-start(bf16[4,128,256]{1,2,0:T(8,128)(2,1)} %copy.76), calls=%async_computation | async-start | bytes 524288 | tf_op jit(solution)/shard_map/all_to_all | solution.py:110
  117.1 3.1 %copy-start = (bf16[128,2048]{1,0:T(8,128)(2,1)S(1)}, bf16[128,2048]{1,0:T(8,128)(2,1)}, u32[]{:S(2)}) copy-start(bf16[128,2048]{1,0:T(8,128)(2,1)} %param.17) | copy-start | bytes 1572868
  117.1 3.1 %copy-start.3 = (f32[2048]{0:T(1024)S(1)}, f32[2048]{0:T(1024)}, u32[]{:S(2)}) copy-start(f32[2048]{0:T(1024)} %param.19) | copy-start | bytes 24580
  120.2 0.7 copy-start.4
  121.7 50.7 %copy-start.6 = (bf16[1,2048,1024]{2,1,0:T(8,128)(2,1)S(1)}, bf16[1,2048,1024]{2,1,0:T(8,128)(2,1)}, u32[]{:S(2)}) copy-start(bf16[1,2048,1024]{2,1,0:T(8,128)(2,1)} %param.23) | copy-start | bytes 12582916
  186.0 4.0 %copy-start.5 = (f32[128,2]{0,1:T(2,128)S(1)}, f32[128,2]{0,1:T(2,128)}, u32[]{:S(2)}) copy-start(f32[128,2]{0,1:T(2,128)} %param.22) | copy-start | bytes 3076
  186.0 52.3 %all-to-all-start.2 = ((bf16[32,16,2048]{2,1,0:T(8,128)(2,1)}), bf16[32,16,2048]{2,1,0:T(8,128)(2,1)S(1)}, u32[]{:S(2)}, u32[]{:S(2)}) async-start(bf16[32,16,2048]{2,1,0:T(8,128)(2,1)} %bitcast.117), calls=%async_computation.2 | async-start | bytes 4194304 | tf_op jit(solution)/shard_map/all_to_all | solution.py:143
Sparse Core Ops, SparseCore 0:
  12.9 42.3 all-gather.1
